TPU v7x, 256 devices: a whole 4x4x8 slice. The times are simulated.
256 devices in a mesh: sp: 32 (over z, x), fs: 4 (over y), tp: 2 (over core).
Axes of the slice: x: 4, y: 4, z: 8, core: 2. Of those that a mesh axis runs over, the one named last changes fastest.
Arguments:
- inputs: bfloat16 [4, 4096, 2048], P('fs', 'sp'), may hold values from -6 to 6
- input_norm_gain: bfloat16 [2048], replicated, may hold values from 0.099609375 to 1.8984375
- receptance_matrix: bfloat16 [2048, 1024], P('fs', 'tp'), may hold values from -0.125 to 0.125
- key_matrix: bfloat16 [2048, 1024], P('fs', 'tp'), may hold values from -0.125 to 0.125
- value_matrix: bfloat16 [2048, 1024], P('fs', 'tp'), may hold values from -0.125 to 0.125
- pooling_input_weight: bfloat16 [2048, 1024], P('fs', 'tp'), may hold values from -0.125 to 0.125
- decay_lower_matrix: bfloat16 [2048, 128], replicated, may hold values from -0.125 to 0.125
- decay_raise_matrix: bfloat16 [2, 64, 1024], P(None, None, 'tp'), may hold values from -1 to 1
- decay_offset_bias: float32 [2, 1024], P(None, 'tp'), may hold values from -13 to -3
- removal_lower_matrix: bfloat16 [2048, 128], replicated, may hold values from -0.125 to 0.125
- removal_raise_matrix: bfloat16 [2, 64, 1024], P(None, None, 'tp'), may hold values from -1 to 1
- removal_rate_bias: float32 [2, 1024], P(None, 'tp'), may hold values from -9 to 1.5
- tempo_scale: float32 [4, 2, 16, 4096], P('fs', None, 'tp', 'sp'), may hold values from 0.3 to 3.2, as said below
- sudden_decay_extra: float32 [4, 2, 16, 4096], P('fs', None, 'tp', 'sp'), may hold values from -2.8 to 0
- head_norm_gain: bfloat16 [1024], P('tp'), may hold values from 0.099609375 to 1.8984375
- group_mixing_weight: bfloat16 [4, 256, 256], P('tp'), may hold values from -0.375 to 0.375
- attention_output_matrix: bfloat16 [2048, 1024], P('fs', 'tp'), may hold values from -0.125 to 0.125
- pooling_output_matrix: bfloat16 [2048, 1024], P('fs', 'tp'), may hold values from -0.125 to 0.125
Outputs:
- mixed_out: bfloat16 [4, 4096, 2048], P('fs', ('sp', 'tp'))
Inputs may be any that keep to these rules, and one draw needn't show every extreme that they name: `tempo_scale`: positive.
All inputs are finite; a program needn't handle non-finite values.
Results may differ from a plain program's by a relative error of at most 0.017.
Values may be sent and summed in bfloat16 or wider, within the bound.
No kernel may reach another device: no remote copies, remote signals or barrier semaphores. Data moves between devices by JAX's collectives and lax.ppermute only.
A program may use at most 128 MiB of HBM per device.

v0:
```python
import jax
import jax.numpy as jnp
from jax import lax
from jax.sharding import Mesh
from jax.sharding import PartitionSpec as P

HEAD = 64
DECAY_RANK = 64
RATE_RANK = 64
POOL_GROUPS = 4
GROUP_WIDTH = 256
SP = ("sp_0", "sp_1")
SP_TP = ("sp_0", "sp_1", "tp")
norm_eps = 1e-06
head_eps = 0.00064
unit_eps = 1e-06
span_len = 32
highest = lax.Precision.HIGHEST


def filled_with(shard, identity):
    return jax.tree.map(
        lambda a, e: jnp.broadcast_to(jnp.asarray(e, a.dtype), a.shape), shard, identity
    )


def prefix_by_axis(shard, axes, combine, identity, reverse):
    before = start = filled_with(shard, identity)
    total = shard
    for axis in reversed(axes):
        peers, here = (lax.axis_size(axis), lax.axis_index(axis))
        pieces = jax.tree.map(
            lambda part, kind: lax.all_gather(part.astype(kind), axis),
            total,
            (jnp.bfloat16, jnp.bfloat16),
        )
        inside, total = (start, start)
        for k in reversed(range(peers)) if reverse else range(peers):
            passed = k > here if reverse else k < here
            total = combine(
                total, jax.tree.map(lambda part, own: part[k].astype(own.dtype), pieces, shard)
            )
            inside = jax.tree.map(lambda new, old: jnp.where(passed, new, old), total, inside)
        before = combine(inside, before)
    return before


def with_halo(cells, sides, width):
    for axis, dim in sides:
        count = lax.axis_size(axis)
        ends = count - 1
        head = lax.slice_in_dim(cells, 0, width, axis=dim)
        tail = lax.slice_in_dim(cells, cells.shape[dim] - width, cells.shape[dim], axis=dim)
        cells = jnp.concatenate(
            [
                lax.ppermute(tail, axis, [(i, (i + 1) % count) for i in range(ends)]),
                cells,
                lax.ppermute(head, axis, [((i + 1) % count, i) for i in range(ends)]),
            ],
            axis=dim,
        )
    return cells


def contract(form, left, right):
    return jnp.einsum(form, left, right, precision=highest)


def matmul(left, right):
    return contract("...ij,...jk->...ik", left, right)


def project(left, weight):
    return jnp.dot(left, weight, preferred_element_type=jnp.float32).astype(jnp.bfloat16)


def against(row_block, weight):
    return lax.dot_general(
        row_block, weight, (((1,), (1,)), ((), ())), preferred_element_type=jnp.float32
    )


def chain_combine(earlier, later):
    return (matmul(earlier[0], later[0]), matmul(earlier[1], later[0]) + later[1])


def unit_inverse(lower):
    result = jnp.eye(lower.shape[-1], dtype=jnp.float32) - lower
    power = lower
    for level in range(4):
        power = matmul(power, power)
        result = result + matmul(result, power)
    return result


def span_terms(logarithm_decay, unit, removal, written, value, recept):
    inner = jnp.cumsum(logarithm_decay, axis=-2)
    last = inner[..., -1:, :]
    ahead = unit * jnp.exp(inner - logarithm_decay)
    shrink = jnp.exp(-inner)
    remove_scaled = removal * shrink
    write_scaled = written * shrink
    query = recept * jnp.exp(inner)
    spots = jnp.arange(span_len)
    strict = spots[:, None] > spots[None, :]
    within = spots[:, None] >= spots[None, :]
    link_remove = jnp.where(strict, contract("...tk,...sk->...ts", ahead, remove_scaled), 0.0)
    link_write = jnp.where(strict, contract("...tk,...sk->...ts", ahead, write_scaled), 0.0)
    read_remove = jnp.where(within, contract("...tk,...sk->...ts", query, remove_scaled), 0.0)
    read_write = jnp.where(within, contract("...tk,...sk->...ts", query, write_scaled), 0.0)
    inverse = unit_inverse(link_remove)
    pull_map = -matmul(inverse, ahead)
    pull_base = -matmul(inverse, matmul(link_write, value))
    tail = jnp.exp(last - inner)
    remove_tail = removal * tail
    write_tail = written * tail
    transfer = jnp.eye(unit.shape[-1], dtype=jnp.float32) * jnp.exp(last) + contract(
        "...sk,...sj->...kj", pull_map, remove_tail
    )
    carried = contract("...sv,...sk->...vk", pull_base, remove_tail) + contract(
        "...sv,...sk->...vk", value, write_tail
    )
    query_eff = query + matmul(read_remove, pull_map)
    local_read = matmul(read_remove, pull_base) + matmul(read_write, value)
    return (query_eff, local_read, transfer, carried)


def shards(
    inputs,
    input_norm_gain,
    receptance_matrix,
    key_matrix,
    value_matrix,
    pooling_input_weight,
    decay_lower_matrix,
    decay_raise_matrix,
    decay_offset_bias,
    removal_lower_matrix,
    removal_raise_matrix,
    removal_rate_bias,
    tempo_scale,
    sudden_decay_extra,
    head_norm_gain,
    group_mixing_weight,
    attention_output_matrix,
    pooling_output_matrix,
):
    recept_full, key_full, value_full, pool_full, attn_full, pool_back = (
        lax.all_gather(receptance_matrix, "fs", axis=0, tiled=True),
        lax.all_gather(key_matrix, "fs", axis=0, tiled=True),
        lax.all_gather(value_matrix, "fs", axis=0, tiled=True),
        lax.all_gather(pooling_input_weight, "fs", axis=0, tiled=True),
        lax.all_gather(attention_output_matrix, "fs", axis=0, tiled=True),
        lax.all_gather(pooling_output_matrix, "fs", axis=0, tiled=True),
    )
    row_block = inputs[0].astype(jnp.float32)
    normed = (
        row_block
        * lax.rsqrt(jnp.mean(row_block * row_block, axis=-1, keepdims=True) + norm_eps)
        * input_norm_gain.astype(jnp.float32)
    ).astype(jnp.bfloat16)
    tokens = normed.shape[0]
    heads = recept_full.shape[1] // HEAD
    blocks = tokens // span_len
    receptance = project(normed, recept_full).astype(jnp.float32).reshape(tokens, heads, HEAD)
    key_rows = project(normed, key_full).astype(jnp.float32).reshape(tokens, heads, HEAD)
    val_rows = project(normed, value_full).astype(jnp.float32).reshape(tokens, heads, HEAD)
    pool_in = project(normed, pool_full)
    decay_act = jnp.tanh(project(normed, decay_lower_matrix).astype(jnp.float32)).astype(
        jnp.bfloat16
    )
    rate_latent = project(normed, removal_lower_matrix)
    unit_keys = key_rows * lax.rsqrt(
        jnp.sum(key_rows * key_rows, axis=-1, keepdims=True) + unit_eps
    )
    decays = []
    removals = []
    writes = []
    for travel_direction in range(2):
        part = decay_act[:, travel_direction * DECAY_RANK : (travel_direction + 1) * DECAY_RANK]
        decay_pre = decay_offset_bias[travel_direction] + jnp.dot(
            part, decay_raise_matrix[travel_direction], preferred_element_type=jnp.float32
        )
        decay_velocity = jnp.exp(-jax.nn.softplus(-decay_pre) - 0.5).reshape(tokens, heads, HEAD)
        decays.append(
            -decay_velocity * tempo_scale[0, travel_direction].T[:, :, None]
            + sudden_decay_extra[0, travel_direction].T[:, :, None]
        )
        latent = rate_latent[:, travel_direction * RATE_RANK : (travel_direction + 1) * RATE_RANK]
        rate = jax.nn.sigmoid(
            removal_rate_bias[travel_direction]
            + jnp.dot(
                latent, removal_raise_matrix[travel_direction], preferred_element_type=jnp.float32
            )
        )
        rate = rate.reshape(tokens, heads, HEAD)
        removals.append(unit_keys * rate)
        writes.append(key_rows * rate)

    def both_ways(forward, backward):
        stacked = jnp.stack([forward, jnp.flip(backward, axis=0)], axis=0)
        return stacked.reshape(2, blocks, span_len, heads, HEAD).transpose(0, 3, 1, 2, 4)

    query_eff, local_read, transfer, carried = span_terms(
        both_ways(decays[0], decays[1]),
        both_ways(unit_keys, unit_keys),
        both_ways(removals[0], removals[1]),
        both_ways(writes[0], writes[1]),
        both_ways(val_rows, val_rows),
        both_ways(receptance, receptance),
    )
    prefix_map, prefix_sum = lax.associative_scan(chain_combine, (transfer, carried), axis=2)
    total_map = prefix_map[:, :, -1]
    total_sum = prefix_sum[:, :, -1]
    identity_map = jnp.broadcast_to(jnp.eye(HEAD, dtype=jnp.float32), total_map.shape[1:])
    empty = jnp.zeros(total_map.shape[1:], jnp.float32)
    ahead_in = prefix_by_axis(
        (total_map[0], total_sum[0]), SP, chain_combine, (identity_map, empty), False
    )
    behind_in = prefix_by_axis(
        (total_map[1], total_sum[1]), SP, chain_combine, (identity_map, empty), True
    )
    incoming = jnp.stack([ahead_in[1], behind_in[1]], axis=0)
    ending = matmul(incoming[:, :, None], prefix_map) + prefix_sum
    starting = jnp.concatenate([incoming[:, :, None], ending[:, :, :-1]], axis=2)
    reads = contract("...tk,...vk->...tv", query_eff, starting) + local_read
    reads = reads.transpose(0, 2, 3, 1, 4).reshape(2, tokens, heads, HEAD)
    readout = reads[0] + jnp.flip(reads[1], axis=0)
    centred = readout - jnp.mean(readout, axis=-1, keepdims=True)
    spread = jnp.mean(centred * centred, axis=-1, keepdims=True)
    attn_out = (centred * lax.rsqrt(spread + head_eps)).reshape(
        tokens, heads * HEAD
    ) * head_norm_gain.astype(jnp.float32)
    attn_out = attn_out.astype(jnp.bfloat16)
    reach = 2 ** (POOL_GROUPS - 1)
    rimmed = with_halo(pool_in, ((SP, 0),), reach).astype(jnp.float32)
    position = lax.axis_index(SP) * tokens + jnp.arange(tokens)
    length = tokens * lax.axis_size(SP)
    running = rimmed
    window_sums = []
    window_counts = []
    for level in range(POOL_GROUPS):
        shift = 2**level
        running = running[:-shift] + running[shift:]
        window_sums.append(running[reach - shift : reach - shift + tokens])
        upper = jnp.minimum(position + shift, length)
        lower = jnp.maximum(position - shift, 0)
        window_counts.append((upper - lower).astype(jnp.float32))
    window_sums = jnp.stack(window_sums, axis=0)
    window_counts = jnp.stack(window_counts, axis=0)
    pool_vals = pool_in.astype(jnp.float32)
    groups_here = pool_in.shape[1] // GROUP_WIDTH
    diffs = []
    for member in range(groups_here):
        group = lax.axis_index("tp") * groups_here + member
        chosen = lax.dynamic_index_in_dim(
            window_sums[:, :, member * GROUP_WIDTH : (member + 1) * GROUP_WIDTH],
            group,
            0,
            keepdims=False,
        )
        count = lax.dynamic_index_in_dim(window_counts, group, 0, keepdims=False)
        diffs.append(
            chosen / count[:, None]
            - pool_vals[:, member * GROUP_WIDTH : (member + 1) * GROUP_WIDTH]
        )
    pool_diff = jnp.concatenate(diffs, axis=1).astype(jnp.bfloat16)
    mixed = [
        jnp.dot(
            pool_diff[:, member * GROUP_WIDTH : (member + 1) * GROUP_WIDTH],
            group_mixing_weight[member],
            preferred_element_type=jnp.float32,
        )
        for member in range(groups_here)
    ]
    pool_out = jnp.concatenate(mixed, axis=1).astype(jnp.bfloat16)
    attn_half, pool_half = (
        lax.all_to_all(attn_out, "tp", split_axis=0, concat_axis=1, tiled=True),
        lax.all_to_all(pool_out, "tp", split_axis=0, concat_axis=1, tiled=True),
    )
    attn_whole, pool_whole = (
        lax.all_gather(attn_full, "tp", axis=1, tiled=True),
        lax.all_gather(pool_back, "tp", axis=1, tiled=True),
    )
    result = against(attn_half, attn_whole) + against(pool_half, pool_whole)
    return result.astype(jnp.bfloat16)[None]


def solution(mesh):
    split = Mesh(
        mesh.devices.reshape(8, 4, mesh.shape["fs"], mesh.shape["tp"]), ("sp_0", "sp_1", "fs", "tp")
    )
    in_specs = (
        P("fs", SP, None),
        P(),
        P("fs", "tp"),
        P("fs", "tp"),
        P("fs", "tp"),
        P("fs", "tp"),
        P(),
        P(None, None, "tp"),
        P(None, "tp"),
        P(),
        P(None, None, "tp"),
        P(None, "tp"),
        P("fs", None, "tp", SP),
        P("fs", None, "tp", SP),
        P("tp"),
        P("tp", None, None),
        P("fs", "tp"),
        P("fs", "tp"),
    )
    out_specs = P("fs", SP_TP, None)
    return jax.shard_map(
        shards, mesh=split, in_specs=in_specs, out_specs=out_specs, check_vma=False
    )
```

profile of v0, /device:TPU:7, one launch (start us, length us, event | category | flops | bytes accessed | tf_op | source)
XLA Modules:
  0.0 448.1 jit_solution(15655499817770157762)
XLA Ops:
  18.1 27.2 %all-gather.19.cloned.1.call-done = bf16[2048,512]{1,0:T(8,128)(2,1)} async-done(((bf16[512,512]{1,0:T(8,128)(2,1)}), bf16[2048,512]{1,0:T(8,128)(2,1)}) %all-gather.19.cloned.1.call-update) | async-done | bytes 2097168 | tf_op jit(solution)/shard_map/all_gather | solution.py:150
  45.3 2.1 fusion.29
  47.6 32.9 %all-gather.21.cloned.1.call-done = bf16[2048,512]{1,0:T(8,128)(2,1)} async-done(((bf16[512,512]{1,0:T(8,128)(2,1)}), bf16[2048,512]{1,0:T(8,128)(2,1)}) %all-gather.21.cloned.1.call-update) | async-done | bytes 2097168 | tf_op jit(solution)/shard_map/all_gather | solution.py:151
  80.5 2.1 fusion.28
  90.6 3.0 fusion.55
  93.6 3.0 convolution_select_fusion.2
  96.6 1.2 fusion.215
  97.8 1.2 fusion.216
  99.0 1.3 convolution_add_fusion.5
  100.3 1.2 fusion.217
  101.5 1.4 convolution_add_fusion.4
  102.9 2.2 fusion.218
  105.1 2.2 convolution_add_fusion.3
  107.3 4.0 convolution_select_fusion.1
  113.4 1.1 copy.129
  114.5 3.2 convolution_add_fusion.2
  117.8 1.8 convolution_negate_fusion.1
  119.6 1.2 fusion.61
  120.8 1.2 convolution_negate_fusion
  122.0 4.2 fusion.46
  126.3 5.0 %multiply_add_fusion = f32[2,8,4,64,64]{4,3,2,1,0:T(8,128)S(1)} fusion(f32[2,8,4,32,64]{4,3,2,1,0:T(8,128)S(1)} %convolution_negate_fusion.1, f32[2,8,4,64]{3,2,1,0:T(4,128)S(1)} %copy-done.59, f32[64,64]{1,0:T(8,128)S(1)} %fusion.167, f32[2,8,4,32,64]{4,1,2,3,0:T(8,128)} %copy-done.15), kind=kOutput, calls=%fused_computation.8 | convolution fusion | flops 101187584 | bytes 2129920 | tf_op jit(solution)/shard_map/...sk,...sj->...kj/dot_general | solution.py:66
  131.3 1.2 fusion.41
  133.3 4.0 convolution_add_fusion.1
  137.3 1.2 convolution_add_fusion.7
  139.2 1.2 pad_add_fusion
  140.4 1.5 fusion.13
  142.6 1.5 convolution_bitcast_fusion.3
  145.7 11.3 %pad.33 = f32[2,8,4,64,64]{4,3,2,1,0:T(8,128)} pad(f32[2,8,2,64,64]{4,3,2,1,0:T(8,128)S(1)} %copy-done.30, f32[]{:T(128)} %constant.27.clone.1), padding=0_0_0x0_0_0x1_0_1x0_0_0x0_0_0 | pad | bytes 1572868 | tf_op jit(solution)/shard_map/pad | solution.py:212
  157.1 11.2 %pad.32 = f32[2,8,4,64,64]{4,3,2,1,0:T(8,128)} pad(f32[2,8,2,64,64]{4,3,2,1,0:T(8,128)S(1)} %pad_maximum_fusion.1, f32[]{:T(128)} %constant.27.clone.1), padding=0_0_0x0_0_0x0_1_1x0_0_0x0_0_0 | pad | bytes 1572868 | tf_op jit(solution)/shard_map/pad | solution.py:212
  168.3 11.2 %pad.28 = f32[2,8,4,64,64]{4,3,2,1,0:T(8,128)} pad(f32[2,8,2,64,64]{4,3,2,1,0:T(8,128)S(1)} %pad_maximum_fusion, f32[]{:T(128)} %constant.27.clone.1), padding=0_0_0x0_0_0x0_1_1x0_0_0x0_0_0 | pad | bytes 1572868 | tf_op jit(solution)/shard_map/pad | solution.py:212
  179.6 16.7 %pad.29 = f32[2,8,4,64,64]{4,3,2,1,0:T(8,128)} pad(f32[2,8,2,64,64]{4,3,2,1,0:T(8,128)} %pad_add_fusion.1, f32[]{:T(128)} %constant.27.clone.1), padding=0_0_0x0_0_0x1_0_1x0_0_0x0_0_0 | pad | bytes 1572868 | tf_op jit(solution)/shard_map/pad | solution.py:212
  196.3 2.2 add_convert_fusion
  198.5 10.7 %all-gather.6 = bf16[4,8,1,64,64]{4,3,2,1,0:T(8,128)(2,1)S(1)} all-gather(bf16[1,8,1,64,64]{4,3,2,1,0:T(8,128)(2,1)S(1)} %get-tuple-element.24), channel_id=8, replica_groups=mesh['sp_0'=8,'sp_1'=4,'fs'=4,'tp'=2] {'sp_1'}, dimensions={0}, use_global_device_ids=true | all-gather | bytes 327680 | tf_op jit(solution)/shard_map/all_gather | solution.py:33
  209.2 1.9 fusion.200
  211.1 11.9 %all-gather.4 = bf16[4,8,1,64,64]{4,3,2,1,0:T(8,128)(2,1)S(1)} all-gather(bf16[1,8,1,64,64]{4,3,2,1,0:T(8,128)(2,1)S(1)} %get-tuple-element.22), channel_id=6, replica_groups=mesh['sp_0'=8,'sp_1'=4,'fs'=4,'tp'=2] {'sp_1'}, dimensions={0}, use_global_device_ids=true | all-gather | bytes 327680 | tf_op jit(solution)/shard_map/all_gather | solution.py:33
  225.7 22.8 %all-gather.7 = bf16[64,64,64]{2,1,0:T(8,128)(2,1)S(1)} all-gather(bf16[8,64,64]{2,1,0:T(8,128)(2,1)S(1)} %get-tuple-element.46), channel_id=9, replica_groups=mesh['sp_0'=8,'sp_1'=4,'fs'=4,'tp'=2] {'sp_0'}, dimensions={0}, use_global_device_ids=true | all-gather | bytes 589824 | tf_op jit(solution)/shard_map/all_gather | solution.py:33
  249.3 22.2 %all-gather.5 = bf16[64,64,64]{2,1,0:T(8,128)(2,1)S(1)} all-gather(bf16[8,64,64]{2,1,0:T(8,128)(2,1)S(1)} %get-tuple-element.48), channel_id=7, replica_groups=mesh['sp_0'=8,'sp_1'=4,'fs'=4,'tp'=2] {'sp_0'}, dimensions={0}, use_global_device_ids=true | all-gather | bytes 589824 | tf_op jit(solution)/shard_map/all_gather | solution.py:33
  273.1 10.5 %all-gather.2 = bf16[4,8,1,64,64]{4,3,2,1,0:T(8,128)(2,1)S(1)} all-gather(bf16[1,8,1,64,64]{4,3,2,1,0:T(8,128)(2,1)S(1)} %get-tuple-element.23), channel_id=4, replica_groups=mesh['sp_0'=8,'sp_1'=4,'fs'=4,'tp'=2] {'sp_1'}, dimensions={0}, use_global_device_ids=true | all-gather | bytes 327680 | tf_op jit(solution)/shard_map/all_gather | solution.py:33
  283.6 10.3 %all-gather = bf16[4,8,1,64,64]{4,3,2,1,0:T(8,128)(2,1)S(1)} all-gather(bf16[1,8,1,64,64]{4,3,2,1,0:T(8,128)(2,1)S(1)} %get-tuple-element.21), channel_id=2, replica_groups=mesh['sp_0'=8,'sp_1'=4,'fs'=4,'tp'=2] {'sp_1'}, dimensions={0}, use_global_device_ids=true | all-gather | bytes 327680 | tf_op jit(solution)/shard_map/all_gather | solution.py:33
  295.9 20.4 %all-gather.3 = bf16[64,64,64]{2,1,0:T(8,128)(2,1)S(1)} all-gather(bf16[8,64,64]{2,1,0:T(8,128)(2,1)S(1)} %get-tuple-element.50), channel_id=5, replica_groups=mesh['sp_0'=8,'sp_1'=4,'fs'=4,'tp'=2] {'sp_0'}, dimensions={0}, use_global_device_ids=true | all-gather | bytes 589824 | tf_op jit(solution)/shard_map/all_gather | solution.py:33
  317.2 21.5 %all-gather.1 = bf16[64,64,64]{2,1,0:T(8,128)(2,1)S(1)} all-gather(bf16[8,64,64]{2,1,0:T(8,128)(2,1)S(1)} %get-tuple-element.52), channel_id=3, replica_groups=mesh['sp_0'=8,'sp_1'=4,'fs'=4,'tp'=2] {'sp_0'}, dimensions={0}, use_global_device_ids=true | all-gather | bytes 589824 | tf_op jit(solution)/shard_map/all_gather | solution.py:33
  345.2 3.0 fusion.30
  348.6 2.1 fusion.14
  350.7 1.8 copy.91
  352.5 1.9 stack.75
  354.4 1.8 rev.22
  356.2 2.0 copy.92
  358.2 1.3 copy.94
  359.5 1.2 copy.93
  360.8 1.3 fusion.17
  363.4 3.1 convolution_select_fusion.3
  366.5 1.2 fusion.221
  367.7 3.1 convolution_select_fusion
  370.8 1.2 convolution_add_fusion.6
  372.1 2.0 convolution_add_fusion.8
  374.1 2.0 convolution_bitcast_fusion
  376.6 3.4 fusion.9
  382.4 2.1 fusion.214
  384.5 1.9 collective-permute-start.1
  386.4 5.5 %collective-permute-start = (bf16[8,512]{1,0:T(8,128)(2,1)S(1)}, bf16[8,512]{1,0:T(8,128)(2,1)S(1)}, u32[]{:S(2)}, u32[]{:S(2)}) collective-permute-start(bf16[8,512]{1,0:T(8,128)(2,1)S(1)} %get-tuple-element.34), channel_id=1, source_target_pairs={{0,8},{8,16},{16,24},{24,32},{32,40},{40,48},{48,56},{56,64},{64,7... | collective-permute-start | bytes 24584 | tf_op jit(solution)/shard_map/ppermute | solution.py:56
  391.9 35.5 %all_to_all.32 = bf16[2,64,512]{2,1,0:T(8,128)(2,1)S(1)} all-to-all(bf16[2,64,512]{2,1,0:T(8,128)(2,1)S(1)} %multiply_convert_fusion), channel_id=1, replica_groups=mesh['sp_0'=8,'sp_1'=4,'fs'=4,'tp'=2] {'tp'}, dimensions={0} | all-to-all | bytes 262144 | tf_op jit(solution)/shard_map/all_to_all | solution.py:278
  429.2 3.9 all_to_all.33
  433.1 3.6 fusion.222
  436.7 4.3 fusion.1
  (306 shorter events, 45.8 us)
Async XLA Ops:
  6.5 5.0 %copy-start = (bf16[2048,128]{1,0:T(8,128)(2,1)S(1)}, bf16[2048,128]{1,0:T(8,128)(2,1)}, u32[]{:S(2)}) copy-start(bf16[2048,128]{1,0:T(8,128)(2,1)} %param.24) | copy-start | bytes 1572868
  6.5 4.7 %copy-start.68 = (f32[2,512]{1,0:T(2,128)S(1)}, f32[2,512]{1,0:T(2,128)}, u32[]{:S(2)}) copy-start(f32[2,512]{1,0:T(2,128)} %param.26) | copy-start | bytes 12292
  6.5 4.7 %copy-start.67 = (bf16[2048]{0:T(1024)(128)(2,1)S(1)}, bf16[2048]{0:T(1024)(128)(2,1)}, u32[]{:S(2)}) copy-start(bf16[2048]{0:T(1024)(128)(2,1)} %param.19) | copy-start | bytes 12292
  6.5 4.7 %copy-start.5 = (bf16[1,128,2048]{2,1,0:T(8,128)(2,1)S(1)}, bf16[1,128,2048]{2,1,0:T(8,128)(2,1)}, u32[]{:S(2)}) copy-start(bf16[1,128,2048]{2,1,0:T(8,128)(2,1)} %param.18) | copy-start | bytes 1572868
  6.5 38.7 %all-gather.19.cloned.1.call-start = ((), (), s32[]{:S(2)}) async-start(), calls=%async_computation.3 | async-start | bytes 2621440 | tf_op jit(solution)/shard_map/all_gather | solution.py:150
  7.3 73.2 %all-gather.21.cloned.1.call-start = ((), (), s32[]{:S(2)}) async-start(), calls=%async_computation.4 | async-start | bytes 2621440 | tf_op jit(solution)/shard_map/all_gather | solution.py:151
  8.0 3.9 copy-start.74
  8.0 337.1 %all-gather.17.cloned.1.call-start = ((), (), s32[]{:S(2)}) async-start(), calls=%async_computation.2 | async-start | bytes 2621440 | tf_op jit(solution)/shard_map/all_gather | solution.py:149
  8.8 339.4 %all-gather.23.cloned.1.call-start = ((), (), s32[]{:S(2)}) async-start(), calls=%async_computation.5 | async-start | bytes 2621440 | tf_op jit(solution)/shard_map/all_gather | solution.py:153
  9.3 372.0 %all-gather.29.cloned.1.call-start = ((), (), s32[]{:S(2)}) async-start(), calls=%async_computation.8 | async-start | bytes 2621440 | tf_op jit(solution)/shard_map/all_gather | solution.py:154
  9.9 2.6 copy-start.65
  9.9 2.6 copy-start.66
  10.0 372.0 %all-gather.27.cloned.1.call-start = ((), (), s32[]{:S(2)}) async-start(), calls=%async_computation.7 | async-start | bytes 2621440 | tf_op jit(solution)/shard_map/all_gather | solution.py:152
  10.5 422.6 %all-gather.25.cloned.1.call-start = ((), (), s32[]{:S(2)}) async-start(), calls=%async_computation.6 | async-start | bytes 6291456 | tf_op jit(solution)/shard_map/all_gather | solution.py:282
  11.5 69.0 %copy-start.62 = (f32[128]{0:T(128)}, f32[128]{0:T(128)S(1)}, u32[]{:S(2)}) copy-start(f32[128]{0:T(128)S(1)} %add_rsqrt_fusion.2) | copy-start | bytes 1540
  15.0 1.9 copy-start.72
  93.6 4.2 copy-start.9
  93.6 13.7 %copy-start.7 = (f32[2,8,4,32,64]{4,1,2,3,0:T(8,128)}, f32[2,8,4,32,64]{4,1,2,3,0:T(8,128)S(1)}, u32[]{:S(2)}) copy-start(f32[2,8,4,32,64]{4,1,2,3,0:T(8,128)S(1)} %get-tuple-element.12) | copy-start | bytes 1572868
  93.6 28.4 %copy-start.15 = (f32[2,8,4,32,64]{4,1,2,3,0:T(8,128)}, f32[2,8,4,32,64]{4,1,2,3,0:T(8,128)S(1)}, u32[]{:S(2)}) copy-start(f32[2,8,4,32,64]{4,1,2,3,0:T(8,128)S(1)} %get-tuple-element.16) | copy-start | bytes 1572868
  114.5 17.9 %copy-start.22 = (f32[1,4,32,8,64]{4,2,1,3,0:T(8,128)}, f32[1,4,32,8,64]{4,2,1,3,0:T(8,128)S(1)}, u32[]{:S(2)}) copy-start(f32[1,4,32,8,64]{4,2,1,3,0:T(8,128)S(1)} %copy.129) | copy-start | bytes 786436
  117.8 1.8 copy-start.20
  119.6 6.7 %copy-start.11 = (f32[2,8,4,32,64]{4,3,2,1,0:T(8,128)}, f32[2,8,4,32,64]{4,3,2,1,0:T(8,128)S(1)}, u32[]{:S(2)}) copy-start(f32[2,8,4,32,64]{4,3,2,1,0:T(8,128)S(1)} %convolution_negate_fusion.1) | copy-start | bytes 1572868
  122.0 4.3 copy-start.13
  122.0 4.3 copy-start.59
  131.3 11.3 %copy-start.2 = (f32[2,8,4,64,64]{4,3,2,1,0:T(8,128)}, f32[2,8,4,64,64]{4,3,2,1,0:T(8,128)S(1)}, u32[]{:S(2)}) copy-start(f32[2,8,4,64,64]{4,3,2,1,0:T(8,128)S(1)} %multiply_add_fusion) | copy-start | bytes 3145732
  131.3 2.0 copy-start.29
  137.3 4.6 %copy-start.16 = (f32[2,8,4,64,64]{4,3,2,1,0:T(8,128)}, f32[2,8,4,64,64]{4,3,2,1,0:T(8,128)S(1)}, u32[]{:S(2)}) copy-start(f32[2,8,4,64,64]{4,3,2,1,0:T(8,128)S(1)} %convolution_add_fusion.1) | copy-start | bytes 3145732
  145.6 11.3 %slice-start.1 = ((f32[2,8,4,64,64]{4,3,2,1,0:T(8,128)}), f32[2,8,1,64,64]{4,3,2,1,0:T(8,128)S(1)}, s32[]{:S(2)}) async-start(f32[2,8,4,64,64]{4,3,2,1,0:T(8,128)} %copy-done.16), calls=%async_computation.11 | async-start | bytes 1048576 | tf_op jit(solution)/shard_map/slice | solution.py:212
  145.7 11.3 %copy-start.53 = (f32[2,8,1,64,64]{4,3,2,1,0:T(8,128)S(1)}, f32[2,8,1,64,64]{4,3,2,1,0:T(8,128)}, u32[]{:S(2)}) copy-start(f32[2,8,1,64,64]{4,3,2,1,0:T(8,128)} %fusion.13) | copy-start | bytes 786436
  157.0 11.2 %slice-start = ((f32[2,8,4,64,64]{4,3,2,1,0:T(8,128)}), f32[2,8,1,64,64]{4,3,2,1,0:T(8,128)S(1)}, s32[]{:S(2)}) async-start(f32[2,8,4,64,64]{4,3,2,1,0:T(8,128)} %copy-done.2), calls=%async_computation.10 | async-start | bytes 1048576 | tf_op jit(solution)/shard_map/slice | solution.py:212
  157.0 11.2 %copy-start.54 = (f32[2,8,1,64,64]{4,3,2,1,0:T(8,128)S(1)}, f32[2,8,1,64,64]{4,3,2,1,0:T(8,128)}, u32[]{:S(2)}) copy-start(f32[2,8,1,64,64]{4,3,2,1,0:T(8,128)} %convolution_bitcast_fusion.3) | copy-start | bytes 786436
  179.6 16.7 %copy-start.3 = (f32[2,8,4,64,64]{4,3,2,1,0:T(8,128)S(1)}, f32[2,8,4,64,64]{4,3,2,1,0:T(8,128)}, u32[]{:S(2)}) copy-start(f32[2,8,4,64,64]{4,3,2,1,0:T(8,128)} %pad.33) | copy-start | bytes 3145732
  196.3 12.9 %copy-start.18 = (f32[2,8,4,64,64]{4,3,2,1,0:T(8,128)S(1)}, f32[2,8,4,64,64]{4,3,2,1,0:T(8,128)}, u32[]{:S(2)}) copy-start(f32[2,8,4,64,64]{4,3,2,1,0:T(8,128)} %pad.28) | copy-start | bytes 3145732
  196.3 12.9 %copy-start.19 = (f32[2,8,4,64,64]{4,3,2,1,0:T(8,128)S(1)}, f32[2,8,4,64,64]{4,3,2,1,0:T(8,128)}, u32[]{:S(2)}) copy-start(f32[2,8,4,64,64]{4,3,2,1,0:T(8,128)} %pad.29) | copy-start | bytes 3145732
  224.5 24.6 %copy-start.33 = (f32[8,64,64]{2,1,0:T(8,128)}, f32[8,64,64]{2,1,0:T(8,128)S(1)}, u32[]{:S(2)}) copy-start(f32[8,64,64]{2,1,0:T(8,128)S(1)} %convolution_add_fusion.19) | copy-start | bytes 393220
  224.8 24.6 %copy-start.34 = (f32[8,64,64]{2,1,0:T(8,128)}, f32[8,64,64]{2,1,0:T(8,128)S(1)}, u32[]{:S(2)}) copy-start(f32[8,64,64]{2,1,0:T(8,128)S(1)} %convolution_add_fusion.18) | copy-start | bytes 393220
  294.4 22.3 %copy-start.45 = (f32[8,64,64]{2,1,0:T(8,128)}, f32[8,64,64]{2,1,0:T(8,128)S(1)}, u32[]{:S(2)}) copy-start(f32[8,64,64]{2,1,0:T(8,128)S(1)} %convolution_add_fusion.33) | copy-start | bytes 393220
  316.4 24.8 %copy-start.26 = (bf16[64,64,64]{2,1,0:T(8,128)(2,1)}, bf16[64,64,64]{2,1,0:T(8,128)(2,1)S(1)}, u32[]{:S(2)}) copy-start(bf16[64,64,64]{2,1,0:T(8,128)(2,1)S(1)} %all-gather.3) | copy-start | bytes 1572868
  338.7 2.5 copy-start.27
  340.1 2.1 copy-start.35
  340.4 1.8 copy-start.37
  342.6 2.5 copy-start.63
  348.2 88.5 %all-gather.31.cloned.1.call-start = ((), (), s32[]{:S(2)}) async-start(), calls=%async_computation.9 | async-start | bytes 6291456 | tf_op jit(solution)/shard_map/all_gather | solution.py:283
  358.1 2.6 copy-start.36
  358.1 2.6 copy-start.38
  358.1 2.6 copy-start.40
  358.1 2.6 copy-start.42
  358.2 2.6 copy-start.44
  358.2 2.6 copy-start.49
  358.2 2.6 copy-start.56
  358.2 4.0 copy-start.57
  359.5 3.1 copy-start.32
  359.5 3.1 copy-start.46
  359.5 3.1 copy-start.55
  360.8 2.2 copy-start.50
  363.4 3.1 copy-start.14
  367.7 3.1 copy-start.21
  367.7 3.1 copy-start.23
  372.0 2.1 copy-start.17
  374.1 2.0 copy-start.4
  381.8 10.1 %copy-start.64 = (f32[512]{0:T(512)S(1)}, f32[512]{0:T(512)}, u32[]{:S(2)}) copy-start(f32[512]{0:T(512)} %convert_element_type.431) | copy-start | bytes 6148
  384.5 43.0 %collective-permute-start.1 = (bf16[8,512]{1,0:T(8,128)(2,1)S(1)}, bf16[8,512]{1,0:T(8,128)(2,1)S(1)}, u32[]{:S(2)}, u32[]{:S(2)}) collective-permute-start(bf16[8,512]{1,0:T(8,128)(2,1)S(1)} %get-tuple-element.35), channel_id=1, source_target_pairs={{8,0},{16,8},{24,16},{32,24},{40,32},{48,40},{56,48},{64,56},{72,6... | collective-permute-start | bytes 24584 | tf_op jit(solution)/shard_map/ppermute | solution.py:58
  386.4 41.1 %collective-permute-start = (bf16[8,512]{1,0:T(8,128)(2,1)S(1)}, bf16[8,512]{1,0:T(8,128)(2,1)S(1)}, u32[]{:S(2)}, u32[]{:S(2)}) collective-permute-start(bf16[8,512]{1,0:T(8,128)(2,1)S(1)} %get-tuple-element.34), channel_id=1, source_target_pairs={{0,8},{8,16},{16,24},{24,32},{32,40},{40,48},{48,56},{56,64},{64,7... | collective-permute-start | bytes 24584 | tf_op jit(solution)/shard_map/ppermute | solution.py:56
  436.7 4.4 copy-start.1
  (24 other events, 28.0 us)
Sparse Core Ops, SparseCore 0:
  9.2 36.0 all-gather.18
  47.1 33.3 all-gather.20
  82.3 33.3 all-gather.16
  117.4 33.3 all-gather.22
  152.5 33.3 all-gather.28
  187.5 33.3 all-gather.26
  348.3 47.0 all-gather.24
  397.2 31.7 all-gather.30
where the time goes:
time: 454 us; the launch traced here: 448 us
  blocking collectives  170 us (37%)
  matrix products  97.3 us (21%)
  local copies, waits for them, and re-layouts  78.8 us (17%)
  waiting for transfers between devices  63.8 us (14%)
  between operations  15.5 us (3%)
  other arithmetic  15 us (3%)
  starting transfers between devices  8.1 us (2%)
    all_gather x8, blocking collectives, prefix_by_axis(): lax.all_gather(part.astype(kind), axis)  130 us
    dot_general x67, matrix products, contract(): return jnp.einsum(form, left, right, precision=highest)  77.8 us
    pad x4, local copies, waits for them, and re-layouts, shards(): lax.associative_scan(chain_combine, (transfer, carried), axis=2)  50.4 us
    all_to_all x1, blocking collectives, shards(): lax.all_to_all(attn_out, 'tp', split_axis=0, concat_axis=1, tiled=True)  35.5 us
    all_gather x1, waiting for transfers between devices, shards(): lax.all_gather(value_matrix, 'fs', axis=0, tiled=True)  32.9 us
    all_gather x1, waiting for transfers between devices, shards(): lax.all_gather(key_matrix, 'fs', axis=0, tiled=True)  27.2 us
    dot_general x6, matrix products, project(): jnp.dot(left, weight, preferred_element_type=jnp.float32)  10 us
    rev x12, local copies, waits for them, and re-layouts, both_ways(): stacked = jnp.stack([forward, jnp.flip(backward, axis=0)], axis=0)  9.63 us
  transfers between devices with their start and end apart: 10, of which 2 were waited for; matrix products, arithmetic and copies ran while one was open for 40% of the time, Pallas kernels for 0%

commit v1 on v0

--- a/solution.py
+++ b/solution.py
@@ -16,6 +16,12 @@
 unit_eps = 1e-06
 span_len = 32
 highest = lax.Precision.HIGHEST
+
+
+def gather_from_all(x, axis, dim):
+    size = lax.axis_size(axis)
+    repeats = [size if d == dim else 1 for d in range(x.ndim)]
+    return lax.all_to_all(jnp.tile(x, repeats), axis, split_axis=dim, concat_axis=dim, tiled=True)
 
 
 def filled_with(shard, identity):
@@ -148,7 +154,7 @@
     recept_full, key_full, value_full, pool_full, attn_full, pool_back = (
         lax.all_gather(receptance_matrix, "fs", axis=0, tiled=True),
         lax.all_gather(key_matrix, "fs", axis=0, tiled=True),
-        lax.all_gather(value_matrix, "fs", axis=0, tiled=True),
+        gather_from_all(value_matrix, "fs", 0),
         lax.all_gather(pooling_input_weight, "fs", axis=0, tiled=True),
         lax.all_gather(attention_output_matrix, "fs", axis=0, tiled=True),
         lax.all_gather(pooling_output_matrix, "fs", axis=0, tiled=True),

time: 454 us -> 429 us (0.945)
  waiting for transfers between devices: 63.8 us -> 32.8 us
  matrix products: 97.3 us -> 90.9 us
  blocking collectives: 170 us -> 175 us
    all_gather x1 -> x0, waiting for transfers between devices: 32.9 us -> none  [shards(): lax.all_gather(value_matrix, 'fs', axis=0, tiled=True)]
    all_to_all x0 -> x1, waiting for transfers between devices: none -> 28.8 us  [gather_from_all(): lax.all_to_all(jnp.tile(x, repeats), axis, split_axis=dim, concat_axis=di...]
    all_gather x1, waiting for transfers between devices: 27.2 us -> 0.71 us  [shards(): lax.all_gather(key_matrix, 'fs', axis=0, tiled=True)]
    dot_general x67, matrix products: 77.8 us -> 71.4 us  [contract(): return jnp.einsum(form, left, right, precision=highest)]
    all_to_all x0 -> x1, starting transfers between devices: none -> 4.59 us  [gather_from_all(): lax.all_to_all(jnp.tile(x, repeats), axis, split_axis=dim, concat_axis=di...]
  transfers between devices with their start and end apart: 10 -> 10, of which waited for: 2 -> 2; matrix products, arithmetic and copies ran while one was open for 40% -> 42% of each run, Pallas kernels for 0% -> 0%
where the time goes in v1:
time: 429 us; the launch traced here: 423 us
  blocking collectives  175 us (41%)
  matrix products  90.9 us (21%)
  local copies, waits for them, and re-layouts  81.4 us (19%)
  waiting for transfers between devices  32.8 us (8%)
  between operations  15.6 us (4%)
  other arithmetic  15.1 us (4%)
  starting transfers between devices  12.6 us (3%)
    all_gather x8, blocking collectives, prefix_by_axis(): lax.all_gather(part.astype(kind), axis)  131 us
    dot_general x67, matrix products, contract(): return jnp.einsum(form, left, right, precision=highest)  71.4 us
    pad x4, local copies, waits for them, and re-layouts, shards(): lax.associative_scan(chain_combine, (transfer, carried), axis=2)  50.4 us
    all_to_all x1, blocking collectives, shards(): lax.all_to_all(attn_out, 'tp', split_axis=0, concat_axis=1, tiled=True)  39.9 us
    all_to_all x1, waiting for transfers between devices, gather_from_all(): lax.all_to_all(jnp.tile(x, repeats), axis, split_axis=dim, concat_axis=di...  28.8 us
    rev x12, local copies, waits for them, and re-layouts, both_ways(): stacked = jnp.stack([forward, jnp.flip(backward, axis=0)], axis=0)  10.5 us
    dot_general x6, matrix products, project(): jnp.dot(left, weight, preferred_element_type=jnp.float32)  10 us
  transfers between devices with their start and end apart: 10, of which 2 were waited for; matrix products, arithmetic and copies ran while one was open for 42% of the time, Pallas kernels for 0%

profile of v1, /device:TPU:7, one launch (start us, length us, event | category | flops | bytes accessed | tf_op | source)
XLA Modules:
  0.0 423.5 jit_solution(6375265814943166524)
XLA Ops:
  9.3 1.6 tile.2
  10.9 4.6 %all-to-all-start = ((bf16[4,512,512]{2,1,0:T(8,128)(2,1)}), bf16[4,512,512]{2,1,0:T(8,128)(2,1)}, u32[]{:S(2)}, u32[]{:S(2)}) async-start(bf16[4,512,512]{2,1,0:T(8,128)(2,1)} %tile.2), calls=%async_computation | async-start | bytes 4194304 | tf_op jit(solution)/shard_map/all_to_all | solution.py:24
  24.8 28.8 %all-to-all-done = bf16[4,512,512]{2,1,0:T(8,128)(2,1)} async-done(((bf16[4,512,512]{2,1,0:T(8,128)(2,1)}), bf16[4,512,512]{2,1,0:T(8,128)(2,1)}, u32[]{:S(2)}, u32[]{:S(2)}) %all-to-all-start) | async-done | bytes 2097184 | tf_op jit(solution)/shard_map/all_to_all | solution.py:24
  53.6 2.1 fusion.30
  57.1 1.3 copy.129
  59.2 2.1 fusion.31
  63.0 1.7 fusion.208
  68.8 2.0 copy.123
  70.7 1.5 copy_multiply_fusion.2
  73.2 3.0 convolution_select_fusion.2
  77.4 1.2 fusion.223
  78.6 1.3 convolution_add_fusion.5
  79.9 1.2 fusion.224
  81.1 1.4 convolution_add_fusion.4
  82.5 1.2 fusion.225
  83.7 1.2 convolution_add_fusion.3
  84.9 3.0 convolution_select_fusion.1
  88.0 1.2 convolution_add_fusion.2
  89.1 1.7 convolution_negate_fusion.1
  90.9 1.2 fusion.65
  93.3 4.2 fusion.50
  97.5 3.7 multiply_add_fusion
  101.3 1.2 fusion.45
  103.2 4.0 convolution_add_fusion.1
  107.3 1.2 convolution_add_fusion.7
  110.4 1.5 fusion.15
  112.5 1.5 convolution_bitcast_fusion.3
  115.6 11.3 %pad.33 = f32[2,8,4,64,64]{4,3,2,1,0:T(8,128)} pad(f32[2,8,2,64,64]{4,3,2,1,0:T(8,128)S(1)} %copy-done.29, f32[]{:T(128)} %constant.27.clone.1), padding=0_0_0x0_0_0x1_0_1x0_0_0x0_0_0 | pad | bytes 1572868 | tf_op jit(solution)/shard_map/pad | solution.py:218
  127.0 11.2 %pad.32 = f32[2,8,4,64,64]{4,3,2,1,0:T(8,128)} pad(f32[2,8,2,64,64]{4,3,2,1,0:T(8,128)S(1)} %pad_maximum_fusion.1, f32[]{:T(128)} %constant.27.clone.1), padding=0_0_0x0_0_0x0_1_1x0_0_0x0_0_0 | pad | bytes 1572868 | tf_op jit(solution)/shard_map/pad | solution.py:218
  138.3 11.2 %pad.28 = f32[2,8,4,64,64]{4,3,2,1,0:T(8,128)} pad(f32[2,8,2,64,64]{4,3,2,1,0:T(8,128)S(1)} %pad_maximum_fusion, f32[]{:T(128)} %constant.27.clone.1), padding=0_0_0x0_0_0x0_1_1x0_0_0x0_0_0 | pad | bytes 1572868 | tf_op jit(solution)/shard_map/pad | solution.py:218
  149.6 16.7 %pad.29 = f32[2,8,4,64,64]{4,3,2,1,0:T(8,128)} pad(f32[2,8,2,64,64]{4,3,2,1,0:T(8,128)} %pad_add_fusion.1, f32[]{:T(128)} %constant.27.clone.1), padding=0_0_0x0_0_0x1_0_1x0_0_0x0_0_0 | pad | bytes 1572868 | tf_op jit(solution)/shard_map/pad | solution.py:218
  166.3 2.2 add_convert_fusion
  168.5 9.9 %all-gather.6 = bf16[4,8,1,64,64]{4,3,2,1,0:T(8,128)(2,1)S(1)} all-gather(bf16[1,8,1,64,64]{4,3,2,1,0:T(8,128)(2,1)S(1)} %get-tuple-element.24), channel_id=8, replica_groups=mesh['sp_0'=8,'sp_1'=4,'fs'=4,'tp'=2] {'sp_1'}, dimensions={0}, use_global_device_ids=true | all-gather | bytes 327680 | tf_op jit(solution)/shard_map/all_gather | solution.py:39
  178.4 1.9 fusion.207
  180.3 11.1 %all-gather.4 = bf16[4,8,1,64,64]{4,3,2,1,0:T(8,128)(2,1)S(1)} all-gather(bf16[1,8,1,64,64]{4,3,2,1,0:T(8,128)(2,1)S(1)} %get-tuple-element.22), channel_id=6, replica_groups=mesh['sp_0'=8,'sp_1'=4,'fs'=4,'tp'=2] {'sp_1'}, dimensions={0}, use_global_device_ids=true | all-gather | bytes 327680 | tf_op jit(solution)/shard_map/all_gather | solution.py:39
  194.2 26.6 %all-gather.7 = bf16[64,64,64]{2,1,0:T(8,128)(2,1)S(1)} all-gather(bf16[8,64,64]{2,1,0:T(8,128)(2,1)S(1)} %get-tuple-element.46), channel_id=9, replica_groups=mesh['sp_0'=8,'sp_1'=4,'fs'=4,'tp'=2] {'sp_0'}, dimensions={0}, use_global_device_ids=true | all-gather | bytes 589824 | tf_op jit(solution)/shard_map/all_gather | solution.py:39
  221.6 21.2 %all-gather.5 = bf16[64,64,64]{2,1,0:T(8,128)(2,1)S(1)} all-gather(bf16[8,64,64]{2,1,0:T(8,128)(2,1)S(1)} %get-tuple-element.48), channel_id=7, replica_groups=mesh['sp_0'=8,'sp_1'=4,'fs'=4,'tp'=2] {'sp_0'}, dimensions={0}, use_global_device_ids=true | all-gather | bytes 589824 | tf_op jit(solution)/shard_map/all_gather | solution.py:39
  244.4 10.5 %all-gather.2 = bf16[4,8,1,64,64]{4,3,2,1,0:T(8,128)(2,1)S(1)} all-gather(bf16[1,8,1,64,64]{4,3,2,1,0:T(8,128)(2,1)S(1)} %get-tuple-element.23), channel_id=4, replica_groups=mesh['sp_0'=8,'sp_1'=4,'fs'=4,'tp'=2] {'sp_1'}, dimensions={0}, use_global_device_ids=true | all-gather | bytes 327680 | tf_op jit(solution)/shard_map/all_gather | solution.py:39
  254.9 9.9 %all-gather = bf16[4,8,1,64,64]{4,3,2,1,0:T(8,128)(2,1)S(1)} all-gather(bf16[1,8,1,64,64]{4,3,2,1,0:T(8,128)(2,1)S(1)} %get-tuple-element.21), channel_id=2, replica_groups=mesh['sp_0'=8,'sp_1'=4,'fs'=4,'tp'=2] {'sp_1'}, dimensions={0}, use_global_device_ids=true | all-gather | bytes 327680 | tf_op jit(solution)/shard_map/all_gather | solution.py:39
  266.8 20.6 %all-gather.3 = bf16[64,64,64]{2,1,0:T(8,128)(2,1)S(1)} all-gather(bf16[8,64,64]{2,1,0:T(8,128)(2,1)S(1)} %get-tuple-element.50), channel_id=5, replica_groups=mesh['sp_0'=8,'sp_1'=4,'fs'=4,'tp'=2] {'sp_0'}, dimensions={0}, use_global_device_ids=true | all-gather | bytes 589824 | tf_op jit(solution)/shard_map/all_gather | solution.py:39
  288.3 21.5 %all-gather.1 = bf16[64,64,64]{2,1,0:T(8,128)(2,1)S(1)} all-gather(bf16[8,64,64]{2,1,0:T(8,128)(2,1)S(1)} %get-tuple-element.52), channel_id=3, replica_groups=mesh['sp_0'=8,'sp_1'=4,'fs'=4,'tp'=2] {'sp_0'}, dimensions={0}, use_global_device_ids=true | all-gather | bytes 589824 | tf_op jit(solution)/shard_map/all_gather | solution.py:39
  316.2 3.0 fusion.32
  319.6 2.1 fusion.16
  321.7 1.8 copy.91
  323.5 1.9 stack.75
  325.4 1.8 rev.22
  327.2 2.0 copy.92
  329.2 1.3 copy.94
  330.5 1.2 copy.93
  331.8 1.3 fusion.19
  334.4 3.1 convolution_select_fusion.3
  337.5 1.2 fusion.228
  338.7 3.1 convolution_select_fusion
  341.8 1.2 convolution_add_fusion.6
  343.1 2.0 convolution_add_fusion.8
  345.1 2.0 convolution_bitcast_fusion
  347.6 3.4 fusion.9
  353.4 2.1 fusion.221
  355.5 1.9 collective-permute-start.1
  357.4 5.5 %collective-permute-start = (bf16[8,512]{1,0:T(8,128)(2,1)S(1)}, bf16[8,512]{1,0:T(8,128)(2,1)S(1)}, u32[]{:S(2)}, u32[]{:S(2)}) collective-permute-start(bf16[8,512]{1,0:T(8,128)(2,1)S(1)} %get-tuple-element.34), channel_id=1, source_target_pairs={{0,8},{8,16},{16,24},{24,32},{32,40},{40,48},{48,56},{56,64},{64,7... | collective-permute-start | bytes 24584 | tf_op jit(solution)/shard_map/ppermute | solution.py:62
  363.0 39.9 %all_to_all.41 = bf16[2,64,512]{2,1,0:T(8,128)(2,1)S(1)} all-to-all(bf16[2,64,512]{2,1,0:T(8,128)(2,1)S(1)} %multiply_convert_fusion), channel_id=1, replica_groups=mesh['sp_0'=8,'sp_1'=4,'fs'=4,'tp'=2] {'tp'}, dimensions={0} | all-to-all | bytes 262144 | tf_op jit(solution)/shard_map/all_to_all | solution.py:284
  404.6 3.9 all_to_all.42
  408.5 3.6 fusion.229
  412.1 4.3 %fusion.1 = bf16[1,64,2048]{2,1,0:T(8,128)(2,1)} fusion(f32[64,2048]{1,0:T(8,128)S(1)} %fusion.229, bf16[64,1024]{1,0:T(8,128)(2,1)S(1)} %bitcast.409, bf16[2048,1024]{1,0:T(8,128)(2,1)} %all-gather.28.cloned.1.call-done), kind=kOutput, calls=%fused_computation.2 | convolution fusion | flops 268697600 | bytes 5111808 | tf_op jit(solution)/shard_map/dot_general | solution.py:84
  (308 shorter events, 48.2 us)
Async XLA Ops:
  6.5 9.9 %copy-start = (bf16[2048,128]{1,0:T(8,128)(2,1)S(1)}, bf16[2048,128]{1,0:T(8,128)(2,1)}, u32[]{:S(2)}) copy-start(bf16[2048,128]{1,0:T(8,128)(2,1)} %param.24) | copy-start | bytes 1572868
  6.5 2.8 copy-start.58
  6.5 52.6 %all-gather.18.cloned.1.call-start = ((), (), s32[]{:S(2)}) async-start(), calls=%async_computation.4 | async-start | bytes 2621440 | tf_op jit(solution)/shard_map/all_gather | solution.py:156
  7.3 308.9 %all-gather.16.cloned.1.call-start = ((), (), s32[]{:S(2)}) async-start(), calls=%async_computation.3 | async-start | bytes 2621440 | tf_op jit(solution)/shard_map/all_gather | solution.py:155
  8.0 311.1 %all-gather.20.cloned.1.call-start = ((), (), s32[]{:S(2)}) async-start(), calls=%async_computation.5 | async-start | bytes 2621440 | tf_op jit(solution)/shard_map/all_gather | solution.py:159
  8.7 343.6 %all-gather.26.cloned.1.call-start = ((), (), s32[]{:S(2)}) async-start(), calls=%async_computation.8 | async-start | bytes 2621440 | tf_op jit(solution)/shard_map/all_gather | solution.py:160
  10.9 5.3 %copy-start.69 = (f32[2,512]{1,0:T(2,128)S(1)}, f32[2,512]{1,0:T(2,128)}, u32[]{:S(2)}) copy-start(f32[2,512]{1,0:T(2,128)} %param.26) | copy-start | bytes 12292
  10.9 5.4 %copy-start.68 = (bf16[2048]{0:T(1024)(128)(2,1)S(1)}, bf16[2048]{0:T(1024)(128)(2,1)}, u32[]{:S(2)}) copy-start(bf16[2048]{0:T(1024)(128)(2,1)} %param.19) | copy-start | bytes 12292
  10.9 5.4 %copy-start.5 = (bf16[1,128,2048]{2,1,0:T(8,128)(2,1)S(1)}, bf16[1,128,2048]{2,1,0:T(8,128)(2,1)}, u32[]{:S(2)}) copy-start(bf16[1,128,2048]{2,1,0:T(8,128)(2,1)} %param.18) | copy-start | bytes 1572868
  10.9 42.7 %all-to-all-start = ((bf16[4,512,512]{2,1,0:T(8,128)(2,1)}), bf16[4,512,512]{2,1,0:T(8,128)(2,1)}, u32[]{:S(2)}, u32[]{:S(2)}) async-start(bf16[4,512,512]{2,1,0:T(8,128)(2,1)} %tile.2), calls=%async_computation | async-start | bytes 4194304 | tf_op jit(solution)/shard_map/all_to_all | solution.py:24
  15.5 2.0 copy-start.66
  15.5 2.0 copy-start.67
  15.5 337.5 %all-gather.24.cloned.1.call-start = ((), (), s32[]{:S(2)}) async-start(), calls=%async_computation.7 | async-start | bytes 2621440 | tf_op jit(solution)/shard_map/all_gather | solution.py:158
  16.1 392.3 %all-gather.22.cloned.1.call-start = ((), (), s32[]{:S(2)}) async-start(), calls=%async_computation.6 | async-start | bytes 6291456 | tf_op jit(solution)/shard_map/all_gather | solution.py:288
  16.5 42.7 %copy-start.63 = (f32[128]{0:T(128)}, f32[128]{0:T(128)S(1)}, u32[]{:S(2)}) copy-start(f32[128]{0:T(128)S(1)} %add_rsqrt_fusion.2) | copy-start | bytes 1540
  20.7 2.2 copy-start.73
  21.9 33.8 %copy-start.25 = (f32[1,4,32,8,64]{4,3,1,2,0:T(8,128)}, f32[1,4,32,8,64]{4,3,1,2,0:T(8,128)S(1)}, u32[]{:S(2)}) copy-start(f32[1,4,32,8,64]{4,3,1,2,0:T(8,128)S(1)} %fusion.77) | copy-start | bytes 786436
  57.1 33.8 %copy-start.19 = (f32[128,8,64]{2,0,1:T(8,128)}, f32[128,8,64]{2,0,1:T(8,128)S(1)}, u32[]{:S(2)}) copy-start(f32[128,8,64]{2,0,1:T(8,128)S(1)} %copy.128) | copy-start | bytes 786436
  58.5 32.4 %copy-start.22 = (f32[1,4,32,8,64]{4,2,1,3,0:T(8,128)}, f32[1,4,32,8,64]{4,2,1,3,0:T(8,128)S(1)}, u32[]{:S(2)}) copy-start(f32[1,4,32,8,64]{4,2,1,3,0:T(8,128)S(1)} %copy.129) | copy-start | bytes 786436
  67.9 4.4 %copy-start.26 = (f32[1,4,32,8,64]{4,3,1,2,0:T(8,128)S(1)}, f32[1,4,32,8,64]{4,3,1,2,0:T(8,128)}, u32[]{:S(2)}) copy-start(f32[1,4,32,8,64]{4,3,1,2,0:T(8,128)} %copy-done.25) | copy-start | bytes 786436
  73.2 4.2 copy-start.9
  73.2 11.7 %copy-start.7 = (f32[2,8,4,32,64]{4,1,2,3,0:T(8,128)}, f32[2,8,4,32,64]{4,1,2,3,0:T(8,128)S(1)}, u32[]{:S(2)}) copy-start(f32[2,8,4,32,64]{4,1,2,3,0:T(8,128)S(1)} %get-tuple-element.12) | copy-start | bytes 1572868
  90.9 6.6 %copy-start.11 = (f32[2,8,4,32,64]{4,3,2,1,0:T(8,128)}, f32[2,8,4,32,64]{4,3,2,1,0:T(8,128)S(1)}, u32[]{:S(2)}) copy-start(f32[2,8,4,32,64]{4,3,2,1,0:T(8,128)S(1)} %convolution_negate_fusion.1) | copy-start | bytes 1572868
  93.3 4.2 %copy-start.13 = (f32[2,8,4,32,64]{4,3,2,1,0:T(8,128)}, f32[2,8,4,32,64]{4,3,2,1,0:T(8,128)S(1)}, u32[]{:S(2)}) copy-start(f32[2,8,4,32,64]{4,3,2,1,0:T(8,128)S(1)} %convolution_negate_fusion) | copy-start | bytes 1572868
  93.3 4.2 %copy-start.60 = (f32[2,8,4,64]{3,2,1,0:T(4,128)S(1)}, f32[2,8,4,64]{3,2,1,0:T(4,128)}, u32[]{:S(2)}) copy-start(f32[2,8,4,64]{3,2,1,0:T(4,128)} %copy.115) | copy-start | bytes 49156
  101.3 11.3 %copy-start.2 = (f32[2,8,4,64,64]{4,3,2,1,0:T(8,128)}, f32[2,8,4,64,64]{4,3,2,1,0:T(8,128)S(1)}, u32[]{:S(2)}) copy-start(f32[2,8,4,64,64]{4,3,2,1,0:T(8,128)S(1)} %multiply_add_fusion) | copy-start | bytes 3145732
  101.3 1.9 copy-start.23
  107.3 4.6 %copy-start.15 = (f32[2,8,4,64,64]{4,3,2,1,0:T(8,128)}, f32[2,8,4,64,64]{4,3,2,1,0:T(8,128)S(1)}, u32[]{:S(2)}) copy-start(f32[2,8,4,64,64]{4,3,2,1,0:T(8,128)S(1)} %convolution_add_fusion.1) | copy-start | bytes 3145732
  115.6 11.3 %slice-start.1 = ((f32[2,8,4,64,64]{4,3,2,1,0:T(8,128)}), f32[2,8,1,64,64]{4,3,2,1,0:T(8,128)S(1)}, s32[]{:S(2)}) async-start(f32[2,8,4,64,64]{4,3,2,1,0:T(8,128)} %copy-done.15), calls=%async_computation.11 | async-start | bytes 1048576 | tf_op jit(solution)/shard_map/slice | solution.py:218
  115.6 11.3 %copy-start.53 = (f32[2,8,1,64,64]{4,3,2,1,0:T(8,128)S(1)}, f32[2,8,1,64,64]{4,3,2,1,0:T(8,128)}, u32[]{:S(2)}) copy-start(f32[2,8,1,64,64]{4,3,2,1,0:T(8,128)} %fusion.15) | copy-start | bytes 786436
  127.0 11.2 %slice-start = ((f32[2,8,4,64,64]{4,3,2,1,0:T(8,128)}), f32[2,8,1,64,64]{4,3,2,1,0:T(8,128)S(1)}, s32[]{:S(2)}) async-start(f32[2,8,4,64,64]{4,3,2,1,0:T(8,128)} %copy-done.2), calls=%async_computation.10 | async-start | bytes 1048576 | tf_op jit(solution)/shard_map/slice | solution.py:218
  127.0 11.2 %copy-start.54 = (f32[2,8,1,64,64]{4,3,2,1,0:T(8,128)S(1)}, f32[2,8,1,64,64]{4,3,2,1,0:T(8,128)}, u32[]{:S(2)}) copy-start(f32[2,8,1,64,64]{4,3,2,1,0:T(8,128)} %convolution_bitcast_fusion.3) | copy-start | bytes 786436
  149.6 16.7 %copy-start.3 = (f32[2,8,4,64,64]{4,3,2,1,0:T(8,128)S(1)}, f32[2,8,4,64,64]{4,3,2,1,0:T(8,128)}, u32[]{:S(2)}) copy-start(f32[2,8,4,64,64]{4,3,2,1,0:T(8,128)} %pad.33) | copy-start | bytes 3145732
  166.3 12.1 %copy-start.17 = (f32[2,8,4,64,64]{4,3,2,1,0:T(8,128)S(1)}, f32[2,8,4,64,64]{4,3,2,1,0:T(8,128)}, u32[]{:S(2)}) copy-start(f32[2,8,4,64,64]{4,3,2,1,0:T(8,128)} %pad.28) | copy-start | bytes 3145732
  166.3 12.1 %copy-start.18 = (f32[2,8,4,64,64]{4,3,2,1,0:T(8,128)S(1)}, f32[2,8,4,64,64]{4,3,2,1,0:T(8,128)}, u32[]{:S(2)}) copy-start(f32[2,8,4,64,64]{4,3,2,1,0:T(8,128)} %pad.29) | copy-start | bytes 3145732
  192.9 28.4 %copy-start.32 = (f32[8,64,64]{2,1,0:T(8,128)}, f32[8,64,64]{2,1,0:T(8,128)S(1)}, u32[]{:S(2)}) copy-start(f32[8,64,64]{2,1,0:T(8,128)S(1)} %convolution_add_fusion.19) | copy-start | bytes 393220
  193.2 28.4 %copy-start.33 = (f32[8,64,64]{2,1,0:T(8,128)}, f32[8,64,64]{2,1,0:T(8,128)S(1)}, u32[]{:S(2)}) copy-start(f32[8,64,64]{2,1,0:T(8,128)S(1)} %convolution_add_fusion.18) | copy-start | bytes 393220
  265.3 22.4 %copy-start.44 = (f32[8,64,64]{2,1,0:T(8,128)}, f32[8,64,64]{2,1,0:T(8,128)S(1)}, u32[]{:S(2)}) copy-start(f32[8,64,64]{2,1,0:T(8,128)S(1)} %convolution_add_fusion.33) | copy-start | bytes 393220
  287.5 24.8 %copy-start.27 = (bf16[64,64,64]{2,1,0:T(8,128)(2,1)}, bf16[64,64,64]{2,1,0:T(8,128)(2,1)S(1)}, u32[]{:S(2)}) copy-start(bf16[64,64,64]{2,1,0:T(8,128)(2,1)S(1)} %all-gather.3) | copy-start | bytes 1572868
  309.8 2.5 copy-start.28
  311.1 2.1 copy-start.34
  313.7 2.5 copy-start.64
  319.2 92.9 %all-gather.28.cloned.1.call-start = ((), (), s32[]{:S(2)}) async-start(), calls=%async_computation.9 | async-start | bytes 6291456 | tf_op jit(solution)/shard_map/all_gather | solution.py:289
  329.2 2.6 copy-start.35
  329.2 2.6 copy-start.37
  329.2 2.6 copy-start.39
  329.2 2.6 copy-start.41
  329.2 2.6 copy-start.43
  329.2 2.6 copy-start.48
  329.2 2.6 copy-start.56
  329.2 4.0 copy-start.57
  330.5 3.1 copy-start.31
  330.5 3.1 copy-start.45
  330.5 3.1 copy-start.55
  331.8 2.2 copy-start.49
  334.4 3.1 copy-start.14
  338.7 3.1 copy-start.21
  338.7 3.1 copy-start.24
  343.1 2.1 copy-start.16
  345.1 2.0 copy-start.4
  352.8 10.1 %copy-start.65 = (f32[512]{0:T(512)S(1)}, f32[512]{0:T(512)}, u32[]{:S(2)}) copy-start(f32[512]{0:T(512)} %convert_element_type.442) | copy-start | bytes 6148
  355.5 47.3 %collective-permute-start.1 = (bf16[8,512]{1,0:T(8,128)(2,1)S(1)}, bf16[8,512]{1,0:T(8,128)(2,1)S(1)}, u32[]{:S(2)}, u32[]{:S(2)}) collective-permute-start(bf16[8,512]{1,0:T(8,128)(2,1)S(1)} %get-tuple-element.35), channel_id=1, source_target_pairs={{8,0},{16,8},{24,16},{32,24},{40,32},{48,40},{56,48},{64,56},{72,6... | collective-permute-start | bytes 24584 | tf_op jit(solution)/shard_map/ppermute | solution.py:64
  357.4 45.4 %collective-permute-start = (bf16[8,512]{1,0:T(8,128)(2,1)S(1)}, bf16[8,512]{1,0:T(8,128)(2,1)S(1)}, u32[]{:S(2)}, u32[]{:S(2)}) collective-permute-start(bf16[8,512]{1,0:T(8,128)(2,1)S(1)} %get-tuple-element.34), channel_id=1, source_target_pairs={{0,8},{8,16},{16,24},{24,32},{32,40},{40,48},{48,56},{56,64},{64,7... | collective-permute-start | bytes 24584 | tf_op jit(solution)/shard_map/ppermute | solution.py:62
  412.1 4.4 %copy-start.1 = (bf16[2048,128]{1,0:T(8,128)(2,1)S(1)}, bf16[2048,128]{1,0:T(8,128)(2,1)}, u32[]{:S(2)}) copy-start(bf16[2048,128]{1,0:T(8,128)(2,1)} %param.24) | copy-start | bytes 1572868
  (25 other events, 31.4 us)
Sparse Core Ops, SparseCore 0:
  9.1 49.9 all-gather.17
  61.0 34.2 all-gather.15
  97.1 33.3 all-gather.19
  132.1 33.3 all-gather.25
  167.2 33.3 all-gather.23
  319.3 51.1 all-gather.21
  372.3 31.7 all-gather.27
